TPU v7x, 32 devices: a whole 2x2x4 slice. The times are simulated.
32 devices in a mesh: fs: 16 (over z, y, x), tp: 2 (over core).
Axes of the slice: x: 2, y: 2, z: 4, core: 2. Of those that a mesh axis runs over, the one named last changes fastest.
Arguments:
- inputs: bfloat16 [8192, 2048], P('fs', 'tp'), may hold values from -6 to 6
- hidden_pre: bfloat16 [8192, 4096], P('fs', 'tp'), may hold values from -6 to 6
- norm_input: bfloat16 [8192, 2048], P('fs', 'tp'), may hold values from -48 to 48, as said below
- out_gain: float32 [2048], P('tp'), may hold values from 0.1 to 1.9
- w_up: bfloat16 [2048, 4096], P('tp', 'fs'), may hold values from -0.125 to 0.125
- w_down: bfloat16 [4096, 2048], P('tp', 'fs'), may hold values from -0.09375 to 0.09375
- cotangent: bfloat16 [8192, 2048], P('fs', 'tp'), may hold values from -6 to 6
Outputs:
- grad_input: bfloat16 [8192, 2048], P('fs', 'tp')
- grad_up: float32 [2048, 4096], P('tp', 'fs')
- grad_gain: float32 [2048], P('tp')
Inputs may be any that keep to these rules, and one draw needn't show every extreme that they name: `norm_input`: each token's features are scaled by a factor of that token, and each block of 2048 / 2 features by a factor of that block.
All inputs are finite; a program needn't handle non-finite values.
Results may differ from a plain program's by a relative error of at most 0.0058.
Values may be sent and summed in bfloat16 or wider, within the bound.
A program may use at most 64 MiB of HBM per device.

v0:
```python
import jax
import jax.numpy as jnp
from jax import lax
from jax.sharding import PartitionSpec as P

norm_eps = 1e-06


def on_device(inputs, hidden_pre, norm_input, out_gain, w_up, w_down, cotangent):
    tok_rows = inputs.shape[0]
    width = inputs.shape[1] * lax.axis_size("tp")
    scaled = (tok_rows * lax.axis_size("fs")) ** (-0.5)
    normed = norm_input.astype(jnp.float32)
    upstream = cotangent.astype(jnp.float32)
    weighted = upstream * out_gain
    square_sum, cross_sum = lax.psum(
        (jnp.sum(normed * normed, axis=1), jnp.sum(weighted * normed, axis=1)), "tp"
    )
    inv_rms = lax.rsqrt(square_sum / width + norm_eps)[:, None]
    cross_mean = (cross_sum / width)[:, None]
    d_out = (weighted * inv_rms - normed * inv_rms * inv_rms * inv_rms * cross_mean).astype(
        jnp.bfloat16
    )
    grad_gain = lax.psum(jnp.sum(upstream * normed * inv_rms, axis=0) * scaled, "fs")
    out_full = lax.all_gather(d_out, "tp", axis=1, tiled=True)
    columns = out_full
    d_act = lax.dot_general(
        columns,
        lax.all_gather(w_down, "fs", axis=1, tiled=True),
        (((1,), (1,)), ((), ())),
        preferred_element_type=jnp.float32,
    )
    d_pre = (d_act * 2.0 * jax.nn.relu(hidden_pre.astype(jnp.float32))).astype(jnp.bfloat16)
    hidden_full = lax.all_gather(d_pre, "tp", axis=1, tiled=True)
    columns = hidden_full
    grad_input = lax.dot_general(
        columns,
        lax.all_gather(w_up, "fs", axis=1, tiled=True),
        (((1,), (1,)), ((), ())),
        preferred_element_type=jnp.float32,
    ).astype(jnp.bfloat16)
    columns = hidden_full
    grad_up = lax.psum_scatter(
        lax.dot_general(
            columns, inputs, (((0,), (0,)), ((), ())), preferred_element_type=jnp.float32
        )
        * scaled,
        "fs",
        scatter_dimension=0,
        tiled=True,
    ).T
    return (grad_input, grad_up, grad_gain)


def solution(mesh):
    placed = (
        P("fs", "tp"),
        P("fs", "tp"),
        P("fs", "tp"),
        P("tp"),
        P("tp", "fs"),
        P("tp", "fs"),
        P("fs", "tp"),
    )
    return jax.shard_map(
        on_device,
        mesh=mesh,
        in_specs=placed,
        out_specs=(P("fs", "tp"), P("tp", "fs"), P("tp")),
        check_vma=False,
    )
```

profile of v0, /device:TPU:10, one launch (start us, length us, event | category | flops | bytes accessed | tf_op | source)
XLA Modules:
  0.0 698.5 jit_solution(14168805298749167662)
XLA Ops:
  7.2 0.0 copy-start
  7.2 0.0 copy-start.1
  7.2 0.0 copy-start.2
  7.2 0.0 copy-start.3
  7.2 0.0 all-gather.5.cloned.1.call-start
  7.3 1.7 fusion.3
  8.9 2.5 psum.21
  11.4 2.4 fusion.9
  13.8 2.5 psum.22
  16.3 0.0 copy-done.1
  16.3 0.0 copy-done.2
  16.3 0.0 copy-done.3
  16.3 1.7 fusion.2
  18.0 0.0 all-gather.5.cloned.1.call-update
  18.0 0.0 all-gather.7.cloned.1.call-start
  18.0 0.7 all-gather.7.cloned.1.call-update
  18.7 0.0 all-gather.9.cloned.1.call-start
  18.8 11.3 %all-gather.5.cloned.1.call-done = bf16[512,2048]{1,0:T(8,128)(2,1)} async-done(((bf16[512,1024]{1,0:T(8,128)(2,1)}), bf16[512,2048]{1,0:T(8,128)(2,1)}) %all-gather.5.cloned.1.call-update) | async-done | bytes 2097168 | tf_op jit(solution)/shard_map/all_gather | solution.py:25
  30.1 142.7 %all-gather.7.cloned.1.call-done = bf16[2048,2048]{1,0:T(8,128)(2,1)} async-done(((bf16[2048,128]{1,0:T(8,128)(2,1)}), bf16[2048,2048]{1,0:T(8,128)(2,1)}) %all-gather.7.cloned.1.call-update) | async-done | bytes 8388624 | tf_op jit(solution)/shard_map/all_gather | solution.py:29
  172.8 10.5 %multiply_convert_fusion = bf16[512,2048]{1,0:T(8,128)(2,1)} fusion(bf16[512,2048]{1,0:T(8,128)(2,1)} %param.8, bf16[512,2048]{1,0:T(8,128)(2,1)} %all-gather.5.cloned.1.call-done, bf16[2048,2048]{1,0:T(8,128)(2,1)} %all-gather.7.cloned.1.call-done), kind=kOutput, calls=%fused_computation.1 | convolution fusion | flops 4300210176 | bytes 14680064 | tf_op jit(solution)/shard_map/dot_general | solution.py:27
  183.3 0.0 all-gather.9.cloned.1.call-update
  183.3 0.0 all-gather.11.cloned.1.call-start
  183.4 0.5 all-gather.11.cloned.1.call-update
  183.9 0.0 reduce-scatter.2.cloned.1.call-start
  184.0 14.4 %all-gather.9.cloned.1.call-done = bf16[512,4096]{1,0:T(8,128)(2,1)} async-done(((bf16[512,2048]{1,0:T(8,128)(2,1)}), bf16[512,4096]{1,0:T(8,128)(2,1)}) %all-gather.9.cloned.1.call-update) | async-done | bytes 4194320 | tf_op jit(solution)/shard_map/all_gather | solution.py:34
  198.4 10.4 %broadcast_multiply_fusion = f32[4096,1024]{1,0:T(8,128)} fusion(bf16[512,4096]{1,0:T(8,128)(2,1)} %all-gather.9.cloned.1.call-done, bf16[512,1024]{1,0:T(8,128)(2,1)S(1)} %copy-done), kind=kOutput, calls=%fused_computation | convolution fusion | flops 4299161600 | bytes 22020096 | tf_op jit(solution)/shard_map/dot_general | solution.py:44
  208.8 0.0 reduce-scatter.2.cloned.1.call-update
  208.8 32.1 %psum.23 = f32[1024]{0:T(1024)} all-reduce(f32[1024]{0:T(1024)S(1)} %broadcast_multiply_fusion.1), channel_id=1, replica_groups=mesh['fs'=16,'tp'=2] {'fs'}, use_global_device_ids=true, to_apply=%region_6.7 | all-reduce | flops 1024 | bytes 8192 | tf_op jit(solution)/shard_map/psum | solution.py:24
  240.9 93.3 %all-gather.11.cloned.1.call-done = bf16[1024,4096]{1,0:T(8,128)(2,1)} async-done(((bf16[1024,256]{1,0:T(8,128)(2,1)}), bf16[1024,4096]{1,0:T(8,128)(2,1)}) %all-gather.11.cloned.1.call-update) | async-done | bytes 8388624 | tf_op jit(solution)/shard_map/all_gather | solution.py:38
  334.2 10.2 %convolution_convert_fusion = bf16[512,1024]{1,0:T(8,128)(2,1)} fusion(bf16[512,4096]{1,0:T(8,128)(2,1)} %all-gather.9.cloned.1.call-done, bf16[1024,4096]{1,0:T(8,128)(2,1)} %all-gather.11.cloned.1.call-done), kind=kOutput, calls=%fused_computation.17 | convolution fusion | flops 4295491584 | bytes 13631488 | tf_op jit(solution)/shard_map/dot_general | solution.py:36
  344.4 345.0 %reduce-scatter.2.cloned.1.call-done = f32[256,1024]{1,0:T(8,128)} async-done(((f32[4096,1024]{1,0:T(8,128)}), f32[256,1024]{1,0:T(8,128)}) %reduce-scatter.2.cloned.1.call-update) | async-done | bytes 1048592 | tf_op jit(solution)/shard_map/reduce_scatter | solution.py:43
  689.4 2.5 copy.10
  (4 shorter events, 0.0 us)
Async XLA Ops:
  7.2 191.2 %copy-start = (bf16[512,1024]{1,0:T(8,128)(2,1)S(1)}, bf16[512,1024]{1,0:T(8,128)(2,1)}, u32[]{:S(2)}) copy-start(bf16[512,1024]{1,0:T(8,128)(2,1)} %param.7) | copy-start | bytes 3145732
  7.2 9.1 %copy-start.1 = (bf16[512,1024]{1,0:T(8,128)(2,1)S(1)}, bf16[512,1024]{1,0:T(8,128)(2,1)}, u32[]{:S(2)}) copy-start(bf16[512,1024]{1,0:T(8,128)(2,1)} %param.9) | copy-start | bytes 3145732
  7.2 9.1 %copy-start.2 = (bf16[512,1024]{1,0:T(8,128)(2,1)S(1)}, bf16[512,1024]{1,0:T(8,128)(2,1)}, u32[]{:S(2)}) copy-start(bf16[512,1024]{1,0:T(8,128)(2,1)} %param.13) | copy-start | bytes 3145732
  7.2 9.1 %copy-start.3 = (f32[1024]{0:T(1024)S(1)}, f32[1024]{0:T(1024)}, u32[]{:S(2)}) copy-start(f32[1024]{0:T(1024)} %param.10) | copy-start | bytes 12292
  7.2 22.9 %all-gather.5.cloned.1.call-start = ((), (), s32[]{:S(2)}) async-start(), calls=%async_computation.1 | async-start | bytes 3145728 | tf_op jit(solution)/shard_map/all_gather | solution.py:25
  18.0 154.8 %all-gather.7.cloned.1.call-start = ((), (), s32[]{:S(2)}) async-start(), calls=%async_computation.2 | async-start | bytes 8912896 | tf_op jit(solution)/shard_map/all_gather | solution.py:29
  18.7 179.7 %all-gather.9.cloned.1.call-start = ((), (), s32[]{:S(2)}) async-start(), calls=%async_computation.3 | async-start | bytes 6291456 | tf_op jit(solution)/shard_map/all_gather | solution.py:34
  183.3 150.9 %all-gather.11.cloned.1.call-start = ((), (), s32[]{:S(2)}) async-start(), calls=%async_computation.4 | async-start | bytes 8912896 | tf_op jit(solution)/shard_map/all_gather | solution.py:38
  183.9 505.5 %reduce-scatter.2.cloned.1.call-start = ((), (), s32[]{:S(2)}) async-start(), calls=%async_computation.5 | async-start | bytes 17825792 | tf_op jit(solution)/shard_map/reduce_scatter | solution.py:43
Sparse Core Ops, SparseCore 0:
  18.1 11.9 all-gather.4
  32.8 139.9 all-gather.6
  183.5 14.8 all-gather.8
  201.0 133.2 all-gather.10
  336.4 352.9 reduce-scatter.1
where the time goes:
time: 699 us; the launch traced here: 698 us
  waiting for transfers between devices  608 us (87%)
  blocking collectives  37.1 us (5%)
  matrix products  31 us (4%)
  between operations  13.8 us (2%)
    reduce_scatter x1, waiting for transfers between devices, on_device(): lax.psum_scatter(lax.dot_general(columns, inputs, (((0,), (0,)), ((), ())...  345 us
    all_gather x1, waiting for transfers between devices, on_device(): lax.all_gather(w_down, 'fs', axis=1, tiled=True)  143 us
    all_gather x1, waiting for transfers between devices, on_device(): lax.all_gather(w_up, 'fs', axis=1, tiled=True)  93.3 us
    psum x1, blocking collectives, on_device(): lax.psum(jnp.sum(upstream * normed * inv_rms, axis=0) * scaled, 'fs')  32.1 us
    all_gather x1, waiting for transfers between devices, on_device(): hidden_full = lax.all_gather(d_pre, 'tp', axis=1, tiled=True)  14.4 us
  transfers between devices with their start and end apart: 5, of which 5 were waited for; matrix products, arithmetic and copies ran while one was open for 3% of the time, Pallas kernels for 0%

commit v1 on v0

--- a/solution.py
+++ b/solution.py
@@ -26,7 +26,7 @@
     columns = out_full
     d_act = lax.dot_general(
         columns,
-        lax.all_gather(w_down, "fs", axis=1, tiled=True),
+        jnp.concatenate(lax.all_gather(w_down, "fs"), axis=1),
         (((1,), (1,)), ((), ())),
         preferred_element_type=jnp.float32,
     )

time: 699 us -> 661 us (0.946)
  waiting for transfers between devices: 608 us -> 559 us
  local copies, waits for them, and re-layouts: 2.56 us -> 15.1 us
    all_gather x1, waiting for transfers between devices: 143 us -> 105 us  [on_device(): lax.all_gather(w_down, 'fs')]
    reshape x0 -> x1, local copies, waits for them, and re-layouts: none -> 12.6 us  [on_device(): jnp.concatenate(lax.all_gather(w_down, 'fs'), axis=1)]
    all_gather x1, waiting for transfers between devices: 11.3 us -> 0.01 us  [on_device(): out_full = lax.all_gather(d_out, 'tp', axis=1, tiled=True)]
  transfers between devices with their start and end apart: 5 -> 5, of which waited for: 5 -> 4; matrix products, arithmetic and copies ran while one was open for 3% -> 6% of each run, Pallas kernels for 0% -> 0%
where the time goes in v1:
time: 661 us; the launch traced here: 660 us
  waiting for transfers between devices  559 us (85%)
  blocking collectives  37 us (6%)
  matrix products  30.4 us (5%)
  local copies, waits for them, and re-layouts  15.1 us (2%)
  between operations  13.8 us (2%)
    reduce_scatter x1, waiting for transfers between devices, on_device(): lax.psum_scatter(lax.dot_general(columns, inputs, (((0,), (0,)), ((), ())...  345 us
    all_gather x1, waiting for transfers between devices, on_device(): lax.all_gather(w_down, 'fs')  105 us
    all_gather x1, waiting for transfers between devices, on_device(): lax.all_gather(w_up, 'fs', axis=1, tiled=True)  93.4 us
    psum x1, blocking collectives, on_device(): lax.psum(jnp.sum(upstream * normed * inv_rms, axis=0) * scaled, 'fs')  32 us
    all_gather x1, waiting for transfers between devices, on_device(): hidden_full = lax.all_gather(d_pre, 'tp', axis=1, tiled=True)  14.1 us
  transfers between devices with their start and end apart: 5, of which 4 were waited for; matrix products, arithmetic and copies ran while one was open for 6% of the time, Pallas kernels for 0%

profile of v1, /device:TPU:10, one launch (start us, length us, event | category | flops | bytes accessed | tf_op | source)
XLA Modules:
  0.0 660.5 jit_solution(6248854844904841484)
XLA Ops:
  7.2 0.0 copy-start
  7.2 0.0 copy-start.1
  7.2 0.0 copy-start.2
  7.2 0.0 copy-start.3
  7.2 0.0 all-gather.12.cloned.1.call-start
  7.3 0.7 all-gather.12.cloned.1.call-update
  7.9 0.0 all-gather.6.cloned.1.call-start
  8.0 1.5 fusion.3
  9.5 2.5 psum.21
  12.0 0.0 copy-done.1
  12.0 2.1 fusion.9
  14.1 2.5 psum.22
  16.6 0.0 copy-done.2
  16.6 1.7 fusion.2
  18.2 0.0 all-gather.6.cloned.1.call-update
  18.3 0.0 all-gather.8.cloned.1.call-start
  18.3 104.8 %all-gather.12.cloned.1.call-done = bf16[32768,128]{1,0:T(8,128)(2,1)} async-done(((bf16[2048,128]{1,0:T(8,128)(2,1)}), bf16[32768,128]{1,0:T(8,128)(2,1)}) %all-gather.12.cloned.1.call-update) | async-done | bytes 8388624 | tf_op jit(solution)/shard_map/all_gather | solution.py:29
  123.1 12.6 %copy.12 = bf16[2048,16,128]{0,2,1:T(8,128)(2,1)} copy(bf16[2048,16,128]{2,0,1:T(8,128)(2,1)} %bitcast.11) | data formatting | bytes 16777216 | tf_op jit(solution)/shard_map/reshape | solution.py:29
  135.7 0.0 copy-done.4
  135.7 9.9 %multiply_convert_fusion = bf16[512,2048]{1,0:T(8,128)(2,1)} fusion(bf16[512,2048]{1,0:T(8,128)(2,1)S(1)} %copy-done.4, bf16[512,2048]{1,0:T(8,128)(2,1)} %all-gather.6.cloned.1.call-done, bf16[2048,2048]{0,1:T(8,128)(2,1)} %bitcast.12), kind=kOutput, calls=%fused_computation.1 | convolution fusion | flops 4300210176 | bytes 14680064 | tf_op jit(solution)/shard_map/dot_general | solution.py:27
  145.7 0.0 all-gather.8.cloned.1.call-update
  145.7 0.0 all-gather.10.cloned.1.call-start
  145.8 0.5 all-gather.10.cloned.1.call-update
  146.3 0.0 reduce-scatter.2.cloned.1.call-start
  146.3 14.1 %all-gather.8.cloned.1.call-done = bf16[512,4096]{1,0:T(8,128)(2,1)} async-done(((bf16[512,2048]{1,0:T(8,128)(2,1)}), bf16[512,4096]{1,0:T(8,128)(2,1)}) %all-gather.8.cloned.1.call-update) | async-done | bytes 4194320 | tf_op jit(solution)/shard_map/all_gather | solution.py:34
  160.4 10.3 %broadcast_multiply_fusion = f32[4096,1024]{1,0:T(8,128)} fusion(bf16[512,4096]{1,0:T(8,128)(2,1)} %all-gather.8.cloned.1.call-done, bf16[512,1024]{1,0:T(8,128)(2,1)S(1)} %copy-done), kind=kOutput, calls=%fused_computation | convolution fusion | flops 4299161600 | bytes 22020096 | tf_op jit(solution)/shard_map/dot_general | solution.py:44
  170.7 0.0 reduce-scatter.2.cloned.1.call-update
  170.8 32.0 %psum.23 = f32[1024]{0:T(1024)} all-reduce(f32[1024]{0:T(1024)S(1)} %broadcast_multiply_fusion.1), channel_id=1, replica_groups=mesh['fs'=16,'tp'=2] {'fs'}, use_global_device_ids=true, to_apply=%region_6.7 | all-reduce | flops 1024 | bytes 8192 | tf_op jit(solution)/shard_map/psum | solution.py:24
  202.8 93.4 %all-gather.10.cloned.1.call-done = bf16[1024,4096]{1,0:T(8,128)(2,1)} async-done(((bf16[1024,256]{1,0:T(8,128)(2,1)}), bf16[1024,4096]{1,0:T(8,128)(2,1)}) %all-gather.10.cloned.1.call-update) | async-done | bytes 8388624 | tf_op jit(solution)/shard_map/all_gather | solution.py:38
  296.2 10.1 %convolution_convert_fusion = bf16[512,1024]{1,0:T(8,128)(2,1)} fusion(bf16[512,4096]{1,0:T(8,128)(2,1)} %all-gather.8.cloned.1.call-done, bf16[1024,4096]{1,0:T(8,128)(2,1)} %all-gather.10.cloned.1.call-done), kind=kOutput, calls=%fused_computation.17 | convolution fusion | flops 4295491584 | bytes 13631488 | tf_op jit(solution)/shard_map/dot_general | solution.py:36
  306.4 345.0 %reduce-scatter.2.cloned.1.call-done = f32[256,1024]{1,0:T(8,128)} async-done(((f32[4096,1024]{1,0:T(8,128)}), f32[256,1024]{1,0:T(8,128)}) %reduce-scatter.2.cloned.1.call-update) | async-done | bytes 1048592 | tf_op jit(solution)/shard_map/reduce_scatter | solution.py:43
  651.4 2.5 copy.13
  (7 shorter events, 0.0 us)
Async XLA Ops:
  7.2 153.2 %copy-start = (bf16[512,1024]{1,0:T(8,128)(2,1)S(1)}, bf16[512,1024]{1,0:T(8,128)(2,1)}, u32[]{:S(2)}) copy-start(bf16[512,1024]{1,0:T(8,128)(2,1)} %param.7) | copy-start | bytes 3145732
  7.2 4.8 copy-start.1
  7.2 9.4 %copy-start.2 = (bf16[512,1024]{1,0:T(8,128)(2,1)S(1)}, bf16[512,1024]{1,0:T(8,128)(2,1)}, u32[]{:S(2)}) copy-start(bf16[512,1024]{1,0:T(8,128)(2,1)} %param.13) | copy-start | bytes 3145732
  7.2 9.4 %copy-start.3 = (f32[1024]{0:T(1024)S(1)}, f32[1024]{0:T(1024)}, u32[]{:S(2)}) copy-start(f32[1024]{0:T(1024)} %param.10) | copy-start | bytes 12292
  7.2 115.9 %all-gather.12.cloned.1.call-start = ((), (), s32[]{:S(2)}) async-start(), calls=%async_computation.5 | async-start | bytes 8912896 | tf_op jit(solution)/shard_map/all_gather | solution.py:29
  7.9 127.8 %all-gather.6.cloned.1.call-start = ((), (), s32[]{:S(2)}) async-start(), calls=%async_computation.1 | async-start | bytes 3145728 | tf_op jit(solution)/shard_map/all_gather | solution.py:25
  18.3 142.1 %all-gather.8.cloned.1.call-start = ((), (), s32[]{:S(2)}) async-start(), calls=%async_computation.2 | async-start | bytes 6291456 | tf_op jit(solution)/shard_map/all_gather | solution.py:34
  123.1 12.6 %copy-start.4 = (bf16[512,2048]{1,0:T(8,128)(2,1)S(1)}, bf16[512,2048]{1,0:T(8,128)(2,1)}, u32[]{:S(2)}) copy-start(bf16[512,2048]{1,0:T(8,128)(2,1)} %param.8) | copy-start | bytes 6291460
  145.7 150.5 %all-gather.10.cloned.1.call-start = ((), (), s32[]{:S(2)}) async-start(), calls=%async_computation.3 | async-start | bytes 8912896 | tf_op jit(solution)/shard_map/all_gather | solution.py:38
  146.3 505.1 %reduce-scatter.2.cloned.1.call-start = ((), (), s32[]{:S(2)}) async-start(), calls=%async_computation.4 | async-start | bytes 17825792 | tf_op jit(solution)/shard_map/reduce_scatter | solution.py:43
Sparse Core Ops, SparseCore 0:
  10.8 112.3 all-gather.11
  125.3 10.1 all-gather.5
  145.8 14.5 all-gather.7
  163.0 133.2 all-gather.9
  298.4 352.9 reduce-scatter.1
